TPU v7x, 32 devices: a whole 2x2x4 slice. The times are simulated.
32 devices in a mesh: ep: 4 (over y, x), tp: 8 (over z, core).
Axes of the slice: x: 2, y: 2, z: 4, core: 2. Of those that a mesh axis runs over, the one named last changes fastest.
Arguments:
- query_heads_rows: bfloat16 [2048, 2048], P('ep', 'tp'), may hold values from -9 to 9
- key_heads_rows: bfloat16 [2048, 2048], P('ep', 'tp'), may hold values from -9 to 9
- value_heads_rows: bfloat16 [2048, 2048], P('ep', 'tp'), may hold values from -6 to 6
- write_strength_logit: bfloat16 [16, 2048], P('tp', 'ep'), may hold values from -3.5 to -1
- decay_preactivation: bfloat16 [16, 2048], P('tp', 'ep'), may hold values from -5 to 5
- head_decay_logarithm: float32 [16], P('tp'), may hold values from -20 to -3
- extra_log_decay: float32 [16, 2048], P('tp', 'ep'), may hold values from -0.7 to 0
- output_weight: bfloat16 [2048, 2048], P('tp'), may hold values from -2 to 2
- second_batch_tokens: bfloat16 [4096, 2048], P(('ep', 'tp')), may hold values from -6 to 6
- expert_norm_scale: float32 [2048], replicated, may hold values from 0.1 to 1.9
- expert_choice_index: int32 [4096, 2], P(('ep', 'tp')), may hold values from 0 to 15, as said below
- group_router_weight: float32 [4096], P(('ep', 'tp')), may hold values from 0.25 to 1
- expert_logit_difference: float32 [4096], P(('ep', 'tp')), may hold values from -8 to 8
- expert_gate_weight: bfloat16 [16, 1024, 2048], P('ep', 'tp'), may hold values from -0.125 to 0.125
- expert_up_weight: bfloat16 [16, 1024, 2048], P('ep', 'tp'), may hold values from -0.125 to 0.125
- expert_down_weight: bfloat16 [16, 1024, 2048], P('ep', 'tp'), may hold values from -0.375 to 0.375
Outputs:
- mixer_output_first: bfloat16 [2048, 2048], P(('ep', 'tp'))
- expert_out: bfloat16 [4096, 2048], P(('ep', 'tp'))
Inputs may be any that keep to these rules, and one draw needn't show every extreme that they name: `expert_choice_index`: each row names two different experts of one group, the experts a * 4 to a * 4 + 3 for some a. In the rows of one device (aligned blocks of 128 rows) no expert is named more than 32 times, and in every device's rows some expert is named exactly 32 times.
All inputs are finite; a program needn't handle non-finite values.
Results may differ from a plain program's by a relative error of at most 0.018.
Values may be sent and summed in bfloat16 or wider, within the bound.
A program may use at most 128 MiB of HBM per device.

v0:
```python
import jax
import jax.numpy as jnp
from jax import lax
from jax.sharding import PartitionSpec as P

DK = 128
DV = 128
BLOCK = 64
CAP = 32
EXPERTS = 16
TOPK = 2


precise_setting = lax.Precision.HIGHEST
norm_eps = 1e-06


def prefix(value, axis, join, neutral):
    count, mine = (lax.axis_size(axis), lax.axis_index(axis))
    pieces = jax.tree.map(lambda part: lax.all_gather(part, axis), value)
    subtotal = jax.tree.map(
        lambda part, zero: jnp.full_like(part, 0) + jnp.asarray(zero, part.dtype), value, neutral
    )

    def step(position, subtotal):
        longer = join(subtotal, jax.tree.map(lambda part: part[position], pieces))
        return jax.tree.map(lambda new, old: jnp.where(position < mine, new, old), longer, subtotal)

    return lax.fori_loop(0, count - 1, step, subtotal)


def unit_rows(matrix):
    return matrix * lax.rsqrt(jnp.sum(matrix * matrix, axis=-1, keepdims=True) + norm_eps)


def block_terms(query_block, key_block, value_block, decay_logarithm, strength):
    span_len = query_block.shape[2]
    dim_value = value_block.shape[-1]
    cumulative = jnp.cumsum(decay_logarithm, axis=-1)
    within = jnp.tril(jnp.ones((span_len, span_len), bool))
    strict = jnp.tril(jnp.ones((span_len, span_len), bool), -1)
    spread = cumulative[..., :, None] - cumulative[..., None, :]
    decayed = jnp.where(within, jnp.exp(jnp.where(within, spread, 0.0)), 0.0)
    weighted = key_block * strength[..., None]
    lower_part = jnp.where(
        strict,
        jnp.einsum("hnid,hnjd->hnij", weighted, key_block, precision=precise_setting) * decayed,
        0.0,
    )
    system = lower_part + jnp.eye(span_len, dtype=jnp.float32)
    rhs_cols = jnp.concatenate(
        [value_block * strength[..., None], weighted * jnp.exp(cumulative)[..., None]], axis=-1
    )
    solved = jax.scipy.linalg.solve_triangular(system, rhs_cols, lower=True, unit_diagonal=True)
    updated_values = solved[..., :dim_value]
    delta_corrections = solved[..., dim_value:]
    scores = jnp.where(
        within,
        jnp.einsum("hnid,hnjd->hnij", query_block, key_block, precision=precise_setting) * decayed,
        0.0,
    )
    decayed_queries = query_block * jnp.exp(cumulative)[..., None]
    decayed_keys = key_block * jnp.exp(cumulative[..., -1:] - cumulative)[..., None]
    block_retention = jnp.exp(cumulative[..., -1])
    return (
        decayed_queries,
        decayed_keys,
        updated_values,
        delta_corrections,
        scores,
        block_retention,
    )


def carry_step(recurrent_state, inputs):
    decayed_queries, decayed_keys, updated_values, delta_corrections, scores, block_retention = (
        inputs
    )
    value_updates = updated_values - jnp.einsum(
        "jdb,jbu->jdu", delta_corrections, recurrent_state, precision=precise_setting
    )
    final_output = jnp.einsum(
        "jdb,jbu->jdu", decayed_queries, recurrent_state, precision=precise_setting
    )
    final_output = final_output + jnp.einsum(
        "hcj,hjv->hcv", scores, value_updates, precision=precise_setting
    )
    recurrent_state = recurrent_state * block_retention[:, None, None] + jnp.einsum(
        "rpq,rpd->rqd", decayed_keys, value_updates, precision=precise_setting
    )
    return (recurrent_state, final_output)


def compose(earlier, latter):
    joined_map = jnp.einsum("hij,hjk->hik", latter[0], earlier[0], precision=precise_setting)
    joined_state = (
        jnp.einsum("hij,hjv->hiv", latter[0], earlier[1], precision=precise_setting) + latter[1]
    )
    return (joined_map, joined_state)


def shards(
    query_heads_rows,
    key_heads_rows,
    value_heads_rows,
    write_strength_logit,
    decay_preactivation,
    head_decay_logarithm,
    extra_log_decay,
    output_weight,
    second_batch_tokens,
    expert_norm_scale,
    expert_choice_index,
    group_router_weight,
    expert_logit_difference,
    expert_gate_weight,
    expert_up_weight,
    expert_down_weight,
):
    length = query_heads_rows.shape[0]
    local_heads = head_decay_logarithm.shape[0]
    blocks = length // BLOCK
    width_model = output_weight.shape[1]

    def heads_first(matrix):
        spread_out = matrix.astype(jnp.float32).reshape(length, local_heads, -1).transpose(1, 0, 2)
        return spread_out.reshape(local_heads, blocks, BLOCK, -1)

    query_block = unit_rows(heads_first(query_heads_rows)) * DK ** (-0.5)
    key_block = unit_rows(heads_first(key_heads_rows))
    value_block = heads_first(value_heads_rows)
    strength = jax.nn.sigmoid(write_strength_logit.astype(jnp.float32)).reshape(
        local_heads, blocks, BLOCK
    )
    decay_logarithm = (
        -jnp.exp(head_decay_logarithm)[:, None]
        * jax.nn.softplus(decay_preactivation.astype(jnp.float32))
        + extra_log_decay
    )
    decay_logarithm = decay_logarithm.reshape(local_heads, blocks, BLOCK)
    decayed_queries, decayed_keys, updated_values, delta_corrections, scores, block_retention = (
        block_terms(query_block, key_block, value_block, decay_logarithm, strength)
    )
    fresh_wide = jnp.concatenate(
        [updated_values, jnp.zeros(updated_values.shape[:-1] + (DK,), jnp.float32)], axis=-1
    )
    inputs = tuple(
        (
            jnp.moveaxis(term, 1, 0)
            for term in (
                decayed_queries,
                decayed_keys,
                fresh_wide,
                delta_corrections,
                scores,
                block_retention,
            )
        )
    )
    identity_map = jnp.broadcast_to(jnp.eye(DK, dtype=jnp.float32), (local_heads, DK, DK))
    start_memory = jnp.concatenate(
        [jnp.zeros((local_heads, DK, DV), jnp.float32), identity_map], axis=-1
    )
    end_memory, outputs = lax.scan(carry_step, start_memory, inputs)
    local_output = outputs[..., :DV]
    projection_matrix = outputs[..., DV:]
    carried_end = end_memory[..., :DV]
    transfer = end_memory[..., DV:]
    _, incoming_rows = prefix(
        (transfer, carried_end), "ep", compose, (identity_map, jnp.zeros_like(carried_end))
    )
    attention_result = local_output + jnp.einsum(
        "xtyg,tgd->xtyd", projection_matrix, incoming_rows, precision=precise_setting
    )
    attn_rows = (
        attention_result.transpose(0, 2, 1, 3)
        .reshape(length, local_heads * DV)
        .astype(jnp.bfloat16)
    )
    summed = lax.psum_scatter(
        jnp.dot(attn_rows, output_weight, preferred_element_type=jnp.float32).astype(jnp.bfloat16),
        "tp",
        scatter_dimension=0,
        tiled=True,
    )
    widened = second_batch_tokens.astype(jnp.float32)
    normed = (
        widened
        * lax.rsqrt(jnp.mean(widened * widened, axis=-1, keepdims=True) + norm_eps)
        * expert_norm_scale
    ).astype(jnp.bfloat16)
    own_tokens = second_batch_tokens.shape[0]
    ep_count = lax.axis_size("ep")
    local_experts = EXPERTS // ep_count
    flat_ids = expert_choice_index.reshape(-1)
    one_hot = (flat_ids[:, None] == jnp.arange(EXPERTS, dtype=jnp.int32)[None, :]).astype(jnp.int32)
    slot_rank = jnp.sum((jnp.cumsum(one_hot, axis=0) - one_hot) * one_hot, axis=1)
    slot_index = flat_ids * CAP + slot_rank
    copy_token = jnp.arange(flat_ids.shape[0], dtype=jnp.int32) // TOPK
    slot_token = jnp.full((EXPERTS * CAP,), own_tokens, jnp.int32).at[slot_index].set(copy_token)
    outgoing = jnp.take(normed, slot_token, axis=0, mode="fill", fill_value=0).reshape(
        ep_count, local_experts, CAP, width_model
    )
    arrived = lax.all_to_all(outgoing, "ep", split_axis=0, concat_axis=0, tiled=True)
    gate_piece = lax.all_gather(expert_gate_weight, "tp", axis=1, tiled=True)
    up_piece = lax.all_gather(expert_up_weight, "tp", axis=1, tiled=True)
    down_piece = lax.all_gather(expert_down_weight, "tp", axis=1, tiled=True)
    gating = jnp.einsum("secd,efd->secf", arrived, gate_piece, preferred_element_type=jnp.float32)
    upward = jnp.einsum("secd,efd->secf", arrived, up_piece, preferred_element_type=jnp.float32)
    hidden = (jax.nn.silu(gating) * upward).astype(jnp.bfloat16)
    produced = jnp.einsum("secf,efd->secd", hidden, down_piece, preferred_element_type=jnp.float32)
    returned = lax.all_to_all(
        produced.astype(jnp.bfloat16), "ep", split_axis=0, concat_axis=0, tiled=True
    )
    flat_results = returned.reshape(EXPERTS * CAP, width_model)
    picked = (
        jnp.take(flat_results, slot_index, axis=0)
        .reshape(own_tokens, TOPK, width_model)
        .astype(jnp.float32)
    )
    leading = jax.nn.sigmoid(expert_logit_difference)
    mixing = group_router_weight[:, None] * jnp.stack([leading, 1.0 - leading], axis=-1)
    expert_out = jnp.sum(mixing[..., None] * picked, axis=1).astype(jnp.bfloat16)
    return (summed, expert_out)


def solution(mesh):
    in_specs = (
        P("ep", "tp"),
        P("ep", "tp"),
        P("ep", "tp"),
        P("tp", "ep"),
        P("tp", "ep"),
        P("tp"),
        P("tp", "ep"),
        P("tp", None),
        P(("ep", "tp"), None),
        P(),
        P(("ep", "tp"), None),
        P(("ep", "tp")),
        P(("ep", "tp")),
        P("ep", "tp", None),
        P("ep", "tp", None),
        P("ep", "tp", None),
    )
    out_specs = (P(("ep", "tp"), None), P(("ep", "tp"), None))
    return jax.shard_map(shards, mesh=mesh, in_specs=in_specs, out_specs=out_specs, check_vma=False)
```

profile of v0, /device:TPU:0, one launch (start us, length us, event | category | flops | bytes accessed | tf_op | source)
XLA Modules:
  0.0 520.2 jit_solution(1640668718798541853)
XLA Ops:
  11.6 1.4 scatter_custom_fusion
  13.5 3.3 gather_fusion
  16.9 3.1 broadcast_select_fusion
  20.0 5.6 %all-to-all-start = ((bf16[4,4,32,2048]{3,2,1,0:T(8,128)(2,1)}), bf16[4,4,32,2048]{3,2,1,0:T(8,128)(2,1)S(1)}, u32[]{:S(2)}, u32[]{:S(2)}) async-start(bf16[4,4,32,2048]{3,2,1,0:T(8,128)(2,1)} %broadcast_select_fusion), calls=%async_computation.1 | async-start | bytes 4194304 | tf_op jit(solution)/shard_map/all_to_all | solution.py:204
  29.5 3.0 fusion.52
  32.4 80.0 %custom-call.4 = f32[2,8,1,64,64]{3,4,2,1,0:T(8,128)} custom-call(f32[2,8,1,64,64]{4,3,2,1,0:T(8,128)} %fusion.52), custom_call_target="InvertDiagBlocksLowerTriangular" | custom-call | tf_op jit(solution)/shard_map/jit(_solve_triangular)/vmap(vmap())/triangular_solve | solution.py:54
  114.4 2.0 copy.100
  119.9 2.5 multiply_multiply_fusion
  122.4 1.1 fusion.59
  124.4 1.1 multiply_bitcast_fusion
  125.6 2.0 fusion.50
  127.5 1.1 select_bitcast_fusion
  128.6 48.9 %while.26 = (s32[]{:T(128)}, f32[2,128,256]{2,1,0:T(8,128)S(1)}, f32[8,2,64,256]{3,2,0,1:T(8,128)}, f32[8,2]{1,0:T(8,128)}, f32[8,2,64,128]{3,2,0,1:T(8,128)}, /...) while((s32[]{:T(128)}, f32[2,128,256]{2,1,0:T(8,128)S(1)}, ...), condition=%wide.region_4.5_spmd, body=%wide.region_3.4_spmd.sunk | while | flops 176357376 | bytes 2231425 | solution.py:164
  128.6 1.2 convolution_subtract_fusion.2
  129.9 1.1 fusion.126
  131.0 1.8 fusion.127
  133.5 1.3 convolution_add_fusion.4
  134.7 1.2 convolution_subtract_fusion.2
  136.0 1.1 fusion.126
  137.1 1.8 fusion.127
  139.6 1.3 convolution_add_fusion.4
  140.8 1.2 convolution_subtract_fusion.2
  142.1 1.1 fusion.126
  143.2 1.8 fusion.127
  145.7 1.3 convolution_add_fusion.4
  146.9 1.2 convolution_subtract_fusion.2
  148.2 1.1 fusion.126
  149.3 1.8 fusion.127
  151.8 1.3 convolution_add_fusion.4
  153.1 1.2 convolution_subtract_fusion.2
  154.3 1.1 fusion.126
  155.4 1.8 fusion.127
  157.9 1.3 convolution_add_fusion.4
  159.1 1.2 convolution_subtract_fusion.2
  160.4 1.1 fusion.126
  161.5 1.8 fusion.127
  164.0 1.3 convolution_add_fusion.4
  165.2 1.2 convolution_subtract_fusion.2
  166.5 1.1 fusion.126
  167.6 1.8 fusion.127
  170.1 1.3 convolution_add_fusion.4
  171.4 1.3 convolution_subtract_fusion.2
  172.6 1.1 fusion.126
  173.8 1.8 fusion.127
  176.3 1.3 convolution_add_fusion.4
  177.6 11.2 %all-gather = f32[8,128,128]{2,1,0:T(8,128)} all-gather(f32[2,128,128]{2,1,0:T(8,128)S(1)} %get-tuple-element.243), channel_id=2, replica_groups=mesh['ep'=4,'tp'=8] {'ep'}, dimensions={0}, use_global_device_ids=true | all-gather | bytes 655360 | tf_op jit(solution)/shard_map/all_gather | solution.py:20
  188.8 11.2 %all-gather.1 = f32[8,128,128]{2,1,0:T(8,128)} all-gather(f32[2,128,128]{2,1,0:T(8,128)S(1)} %get-tuple-element.242), channel_id=3, replica_groups=mesh['ep'=4,'tp'=8] {'ep'}, dimensions={0}, use_global_device_ids=true | all-gather | bytes 655360 | tf_op jit(solution)/shard_map/all_gather | solution.py:20
  200.1 4.0 while.27
  200.1 1.2 fusion.130
  201.4 1.2 fusion.130
  202.7 1.2 fusion.130
  204.1 1.8 fusion.55
  206.2 2.1 convolution_convert_fusion
  208.4 12.9 %fusion.26 = f32[4,4,32,1024]{3,2,1,0:T(8,128)} fusion(bf16[4,1024,2048]{2,1,0:T(8,128)(2,1)} %all-gather.8.cloned.1.call-done, bf16[4,4,32,2048]{3,2,1,0:T(8,128)(2,1)S(1)} %all-to-all-done), kind=kOutput, calls=%fused_computation.34 | convolution fusion | flops 2147483648 | bytes 20971520 | tf_op jit(solution)/shard_map/secd,efd->secf/dot_general | solution.py:209
  221.3 93.1 %all-gather.6.cloned.1.call-done = bf16[4,1024,2048]{2,1,0:T(8,128)(2,1)} async-done(((bf16[4,128,2048]{2,1,0:T(8,128)(2,1)}), bf16[4,1024,2048]{2,1,0:T(8,128)(2,1)}) %all-gather.6.cloned.1.call-update) | async-done | bytes 16777232 | tf_op jit(solution)/shard_map/all_gather | solution.py:205
  314.3 13.1 %fusion.36 = bf16[4,4,32,1024]{3,2,0,1:T(8,128)(2,1)} fusion(f32[4,4,32,1024]{3,2,1,0:T(8,128)} %fusion.26, bf16[4,1024,2048]{2,1,0:T(8,128)(2,1)} %all-gather.6.cloned.1.call-done, bf16[4,4,32,2048]{3,2,1,0:T(8,128)(2,1)S(1)} %all-to-all-done), kind=kOutput, calls=%fused_computation.42 | convolution fusion | flops 2150629376 | bytes 22020096 | tf_op jit(solution)/shard_map/secd,efd->secf/dot_general | solution.py:208
  327.4 137.8 %all-gather.10.cloned.1.call-done = bf16[4,1024,2048]{2,1,0:T(8,128)(2,1)} async-done(((bf16[4,128,2048]{2,1,0:T(8,128)(2,1)}), bf16[4,1024,2048]{2,1,0:T(8,128)(2,1)}) %all-gather.10.cloned.1.call-update) | async-done | bytes 16777232 | tf_op jit(solution)/shard_map/all_gather | solution.py:207
  465.3 8.5 %fusion.33 = bf16[4,4,32,2048]{3,2,0,1:T(8,128)(2,1)S(1)} fusion(bf16[4,4,32,1024]{3,2,0,1:T(8,128)(2,1)} %fusion.36, bf16[4,1024,2048]{2,1,0:T(8,128)(2,1)} %all-gather.10.cloned.1.call-done), kind=kOutput, calls=%fused_computation.40 | convolution fusion | flops 2148532224 | bytes 19922944 | tf_op jit(solution)/shard_map/secf,efd->secd/dot_general | solution.py:211
  473.7 1.6 copy.119
  475.3 4.0 all-to-all-start.1
  479.9 24.7 %all-to-all-done.1 = bf16[4,4,32,2048]{3,2,1,0:T(8,128)(2,1)S(1)} async-done(((bf16[4,4,32,2048]{3,2,1,0:T(8,128)(2,1)}), bf16[4,4,32,2048]{3,2,1,0:T(8,128)(2,1)S(1)}, u32[]{:S(2)}, u32[]{:S(2)}) %all-to-all-start.1) | async-done | bytes 2097184 | tf_op jit(solution)/shard_map/all_to_all | solution.py:212
  504.6 2.3 gather_fusion.1
  507.0 1.7 gather.15
  508.7 4.9 multiply_reduce_fusion
  (132 shorter events, 21.3 us)
Async XLA Ops:
  7.2 199.1 %copy-start = (bf16[256,2048]{1,0:T(8,128)(2,1)S(1)}, bf16[256,2048]{1,0:T(8,128)(2,1)}, u32[]{:S(2)}) copy-start(bf16[256,2048]{1,0:T(8,128)(2,1)} %param.27) | copy-start | bytes 3145732
  7.2 201.2 %all-gather.8.cloned.1.call-start = ((), (), s32[]{:S(2)}) async-start(), calls=%async_computation.5 | async-start | bytes 18874368 | tf_op jit(solution)/shard_map/all_gather | solution.py:206
  7.9 1.5 copy-start.11
  7.9 5.2 %copy-start.2 = (bf16[128,2048]{1,0:T(8,128)(2,1)S(1)}, bf16[128,2048]{1,0:T(8,128)(2,1)}, u32[]{:S(2)}) copy-start(bf16[128,2048]{1,0:T(8,128)(2,1)} %param.28) | copy-start | bytes 1572868
  7.9 5.4 %copy-start.14 = (f32[2048]{0:T(1024)S(1)}, f32[2048]{0:T(1024)}, u32[]{:S(2)}) copy-start(f32[2048]{0:T(1024)} %param.29) | copy-start | bytes 24580
  7.9 306.4 %all-gather.6.cloned.1.call-start = ((), (), s32[]{:S(2)}) async-start(), calls=%async_computation.4 | async-start | bytes 18874368 | tf_op jit(solution)/shard_map/all_gather | solution.py:205
  8.7 456.6 %all-gather.10.cloned.1.call-start = ((), (), s32[]{:S(2)}) async-start(), calls=%async_computation.6 | async-start | bytes 18874368 | tf_op jit(solution)/shard_map/all_gather | solution.py:207
  11.0 0.6 copy-start.9
  11.6 1.5 copy-start.17
  20.0 5.6 %copy-start.23 = (f32[2]{0:T(128)S(1)}, f32[2]{0:T(128)}, u32[]{:S(2)}) copy-start(f32[2]{0:T(128)} %param.25) | copy-start | bytes 28
  20.0 5.6 %copy-start.19 = (f32[2,512]{1,0:T(2,128)S(1)}, f32[2,512]{1,0:T(2,128)}, u32[]{:S(2)}) copy-start(f32[2,512]{1,0:T(2,128)} %param.26) | copy-start | bytes 12292
  20.0 5.6 %copy-start.20 = (bf16[2,512]{1,0:T(2,128)(2,1)S(1)}, bf16[2,512]{1,0:T(2,128)(2,1)}, u32[]{:S(2)}) copy-start(bf16[2,512]{1,0:T(2,128)(2,1)} %param.24) | copy-start | bytes 6148
  20.0 5.8 %copy-start.6 = (bf16[512,256]{1,0:T(8,128)(2,1)S(1)}, bf16[512,256]{1,0:T(8,128)(2,1)}, u32[]{:S(2)}) copy-start(bf16[512,256]{1,0:T(8,128)(2,1)} %param.21) | copy-start | bytes 786436
  20.0 188.4 %all-to-all-start = ((bf16[4,4,32,2048]{3,2,1,0:T(8,128)(2,1)}), bf16[4,4,32,2048]{3,2,1,0:T(8,128)(2,1)S(1)}, u32[]{:S(2)}, u32[]{:S(2)}) async-start(bf16[4,4,32,2048]{3,2,1,0:T(8,128)(2,1)} %broadcast_select_fusion), calls=%async_computation.1 | async-start | bytes 4194304 | tf_op jit(solution)/shard_map/all_to_all | solution.py:204
  25.6 488.0 %reduce-scatter.2.cloned.1.call-start = ((), (), s32[]{:S(2)}) async-start(), calls=%async_computation.3 | async-start | bytes 2359296 | tf_op jit(solution)/shard_map/reduce_scatter | solution.py:180
  28.6 0.6 copy-start.15
  28.7 0.8 copy-start.4
  116.8 0.6 copy-start.13
  118.1 4.3 copy-start.7
  122.4 2.0 copy-start.3
  122.4 3.1 copy-start.5
  122.4 3.1 copy-start.8
  122.4 3.1 copy-start.16
  123.6 4.0 copy-start.21
  475.3 4.0 copy-start.10
  475.3 4.2 copy-start.12
  475.3 4.4 copy-start.24
  475.3 4.4 copy-start.22
  475.3 4.6 copy-start.18
  475.3 29.3 %all-to-all-start.1 = ((bf16[4,4,32,2048]{3,2,1,0:T(8,128)(2,1)}), bf16[4,4,32,2048]{3,2,1,0:T(8,128)(2,1)S(1)}, u32[]{:S(2)}, u32[]{:S(2)}) async-start(bf16[4,4,32,2048]{3,2,1,0:T(8,128)(2,1)} %copy.119), calls=%async_computation.2 | async-start | bytes 4194304 | tf_op jit(solution)/shard_map/all_to_all | solution.py:212
  504.6 9.0 %copy-start.1 = (bf16[256,2048]{1,0:T(8,128)(2,1)S(1)}, bf16[256,2048]{1,0:T(8,128)(2,1)}, u32[]{:S(2)}) copy-start(bf16[256,2048]{1,0:T(8,128)(2,1)} %param.27) | copy-start | bytes 3145732
Sparse Core Ops, SparseCore 0:
  9.6 153.7 all-gather.7
  165.0 149.2 all-gather.5
  316.0 149.2 all-gather.9
  468.0 34.1 reduce-scatter.1
where the time goes:
time: 522 us; the launch traced here: 520 us
  waiting for transfers between devices  258 us (49%)
  other arithmetic  98.3 us (19%)
  matrix products  91.2 us (17%)
  local copies, waits for them, and re-layouts  26 us (5%)
  blocking collectives  22.5 us (4%)
  between operations  14.2 us (3%)
  starting transfers between devices  9.7 us (2%)
    all_gather x1, waiting for transfers between devices, shards(): down_piece = lax.all_gather(expert_down_weight, 'tp', axis=1, tiled=True)  138 us
    all_gather x1, waiting for transfers between devices, shards(): gate_piece = lax.all_gather(expert_gate_weight, 'tp', axis=1, tiled=True)  93.1 us
    another operation x2, other arithmetic, block_terms(): jax.scipy.linalg.solve_triangular(system, rhs_cols, lower=True, unit_diag...  80 us
    all_to_all x1, waiting for transfers between devices, shards(): lax.all_to_all(produced.astype(jnp.bfloat16), 'ep', split_axis=0, concat_...  24.7 us
    all_gather x2, blocking collectives, prefix(): pieces = jax.tree.map(lambda part: lax.all_gather(part, axis), value)  22.5 us
    dot_general x8, matrix products, carry_step(): jnp.einsum('hcj,hjv->hcv', scores, value_updates, precision=precise_setting)  14.2 us
    dot_general x1, matrix products, shards(): jnp.einsum('secd,efd->secf', arrived, gate_piece, preferred_element_type=...  13.1 us
    dot_general x1, matrix products, shards(): jnp.einsum('secd,efd->secf', arrived, up_piece, preferred_element_type=jn...  12.9 us
  transfers between devices with their start and end apart: 6, of which 3 were waited for; matrix products, arithmetic and copies ran while one was open for 41% of the time, Pallas kernels for 0%

commit v1 on v0

v1 whole, which is shorter than its diff:
```python
import jax
import jax.numpy as jnp
from jax import lax
from jax.experimental import pallas as pl
from jax.experimental.pallas import tpu as pltpu
from jax.sharding import PartitionSpec as P

DK = 128
DV = 128
CAP = 32
EPG = 4
TOPK = 2


precise_setting = lax.Precision.HIGHEST
norm_eps = 1e-06


def prefix(value, axis, join, neutral):
    count, mine = (lax.axis_size(axis), lax.axis_index(axis))
    pieces = jax.tree.map(lambda part: lax.all_gather(part, axis), value)
    subtotal = jax.tree.map(
        lambda part, zero: jnp.full_like(part, 0) + jnp.asarray(zero, part.dtype), value, neutral
    )

    def step(position, subtotal):
        longer = join(subtotal, jax.tree.map(lambda part: part[position], pieces))
        return jax.tree.map(lambda new, old: jnp.where(position < mine, new, old), longer, subtotal)

    return lax.fori_loop(0, count - 1, step, subtotal)


def unit_rows(matrix):
    return matrix * lax.rsqrt(jnp.sum(matrix * matrix, axis=-1, keepdims=True) + norm_eps)


def mm(a, b, dims=((1,), (0,))):
    return lax.dot_general(
        a, b, (dims, ((), ())), precision=precise_setting, preferred_element_type=jnp.float32
    )


def delta_kernel(q_ref, k_ref, v_ref, strength_ref, decay_ref, local_ref, proj_ref, end_ref):
    heads = strength_ref.shape[0]
    chunk = DK
    chunks = q_ref.shape[0] // chunk
    rows = lax.broadcasted_iota(jnp.int32, (chunk, chunk), 0)
    cols = lax.broadcasted_iota(jnp.int32, (chunk, chunk), 1)
    within = rows >= cols
    eye = jnp.where(rows == cols, 1.0, 0.0)
    parts = []
    for h in range(heads):
        for c in range(chunks):
            at = pl.ds(c * chunk, chunk)
            q = q_ref[at, h * DK : (h + 1) * DK].astype(jnp.float32)
            k = k_ref[at, h * DK : (h + 1) * DK].astype(jnp.float32)
            v = v_ref[at, h * DV : (h + 1) * DV].astype(jnp.float32)
            q = unit_rows(q) * DK ** (-0.5)
            k = unit_rows(k)
            d_row = decay_ref[h : h + 1, c * chunk : (c + 1) * chunk]
            b_row = strength_ref[h : h + 1, c * chunk : (c + 1) * chunk]
            d_col = jnp.sum(jnp.where(rows == cols, d_row, 0.0), axis=1, keepdims=True)
            b_col = jnp.sum(jnp.where(rows == cols, b_row, 0.0), axis=1, keepdims=True)
            cum_col = jnp.sum(jnp.where(within, d_row, 0.0), axis=1, keepdims=True)
            cum_row = jnp.sum(jnp.where(rows <= cols, d_col, 0.0), axis=0, keepdims=True)
            last = cum_col[chunk - 1 : chunk, :]
            decayed = jnp.where(within, jnp.exp(jnp.where(within, cum_col - cum_row, 0.0)), 0.0)
            weighted = k * b_col
            lower = jnp.where(
                rows > cols, mm(weighted, k, ((1,), (1,))) * decayed, 0.0
            )
            scores = mm(q, k, ((1,), (1,))) * decayed
            grown = jnp.exp(cum_col)
            rhs = jnp.concatenate([v * b_col, weighted * grown], axis=1)
            parts.append([lower, scores, rhs, q * grown, k * jnp.exp(last - cum_col), jnp.exp(last)])
    inverses = [None] * len(parts)
    span = 1
    while span < chunk:
        mask = (
            (rows // (2 * span) == cols // (2 * span))
            & (rows // span % 2 == 1)
            & (cols // span % 2 == 0)
        )
        for i, part in enumerate(parts):
            edge = jnp.where(mask, part[0], 0.0)
            if span == 1:
                inverses[i] = eye - edge
            else:
                inverses[i] = inverses[i] - mm(mm(inverses[i], edge), inverses[i])
        span *= 2
    solved = [mm(inverse, part[2]) for inverse, part in zip(inverses, parts)]
    states = [
        jnp.concatenate([jnp.zeros((DK, DV), jnp.float32), eye], axis=1) for _ in range(heads)
    ]
    for c in range(chunks):
        for h in range(heads):
            _, scores, _, queries, keys, retention = parts[h * chunks + c]
            both = solved[h * chunks + c]
            fresh = jnp.concatenate([both[:, :DV], jnp.zeros((chunk, DK), jnp.float32)], axis=1)
            state = states[h]
            updates = fresh - mm(both[:, DV:], state)
            out = mm(queries, state) + mm(scores, updates)
            states[h] = state * retention + mm(keys, updates, ((0,), (0,)))
            at = pl.ds(c * chunk, chunk)
            local_ref[h, at, :] = out[:, :DV]
            proj_ref[h, at, :] = out[:, DV:]
    for h in range(heads):
        end_ref[h] = states[h]


def delta_rule(queries, keys, values, strength, decay_logarithm):
    heads, length = strength.shape
    vmem = pl.BlockSpec(memory_space=pltpu.VMEM)
    f32 = jnp.float32
    return pl.pallas_call(
        delta_kernel,
        out_shape=(
            jax.ShapeDtypeStruct((heads, length, DV), f32),
            jax.ShapeDtypeStruct((heads, length, DK), f32),
            jax.ShapeDtypeStruct((heads, DK, DV + DK), f32),
        ),
        in_specs=[vmem] * 5,
        out_specs=(vmem,) * 3,
        cost_estimate=pl.CostEstimate(
            flops=40 * heads * length * DK * DK * 6, bytes_accessed=4 * 2**20, transcendentals=0
        ),
        compiler_params=pltpu.CompilerParams(vmem_limit_bytes=40 * 2**20),
    )(queries, keys, values, strength, decay_logarithm)


def expert_kernel(x_ref, gate_ref, up_ref, down_ref, out_ref):
    experts, units, width = gate_ref.shape
    x = x_ref[:, :width]
    hidden = []
    for e in range(experts):
        gating = lax.dot_general(
            x, gate_ref[e], (((1,), (1,)), ((), ())), preferred_element_type=jnp.float32
        )
        upward = lax.dot_general(
            x, up_ref[e], (((1,), (1,)), ((), ())), preferred_element_type=jnp.float32
        )
        share = x_ref[:, width + e : width + e + 1].astype(jnp.float32) + x_ref[
            :, width + experts + e : width + experts + e + 1
        ].astype(jnp.float32)
        hidden.append((gating / (1.0 + jnp.exp(-gating)) * upward * share).astype(jnp.bfloat16))
    hidden = jnp.concatenate(hidden, axis=1)
    down = down_ref[...].reshape(experts * units, width)
    out_ref[...] = jnp.dot(hidden, down, preferred_element_type=jnp.float32).astype(jnp.bfloat16)


def expert_layer(rows, gate, up, down, tile):
    count, wide = rows.shape
    experts, units, width = gate.shape
    whole = pl.BlockSpec((experts, units, width), lambda i: (0, 0, 0))
    return pl.pallas_call(
        expert_kernel,
        grid=(count // tile,),
        out_shape=jax.ShapeDtypeStruct((count, width), jnp.bfloat16),
        in_specs=[pl.BlockSpec((tile, wide), lambda i: (i, 0)), whole, whole, whole],
        out_specs=pl.BlockSpec((tile, width), lambda i: (i, 0)),
        cost_estimate=pl.CostEstimate(
            flops=6 * count * experts * units * width,
            bytes_accessed=4 * count * width + 6 * experts * units * width,
            transcendentals=0,
        ),
        compiler_params=pltpu.CompilerParams(vmem_limit_bytes=48 * 2**20),
    )(rows, gate, up, down)


def by_tokens(normed, choice, mixing, gate, up, down, slots):
    ep_count = lax.axis_size("ep")
    local_experts = gate.shape[0]
    tokens, width = normed.shape
    bf16 = jnp.bfloat16
    f32 = jnp.float32
    named = choice[:, :, None] == jnp.arange(ep_count * local_experts, dtype=jnp.int32)
    share = jnp.sum(jnp.where(named, mixing[:, :, None], 0.0), axis=1)
    goes = jnp.any(named, axis=1).reshape(tokens, ep_count, local_experts).any(axis=-1)
    earlier = jnp.tril(jnp.ones((tokens, tokens), bf16), -1)
    rank = jnp.dot(earlier, goes.astype(bf16), preferred_element_type=f32)
    spread = goes[:, :, None] & (rank[:, :, None] == jnp.arange(slots, dtype=f32))
    spread = spread.astype(bf16)
    high = share.astype(bf16)
    low = (share - high.astype(f32)).astype(bf16)
    sent = jnp.einsum("tes,td->esd", spread, normed, preferred_element_type=f32).astype(bf16)
    extra = jnp.concatenate(
        [
            high.reshape(tokens, ep_count, local_experts),
            low.reshape(tokens, ep_count, local_experts),
        ],
        axis=-1,
    )
    extra = jnp.einsum("tes,tex->esx", spread, extra, preferred_element_type=f32).astype(bf16)
    pad = -extra.shape[-1] % 128
    extra = jnp.pad(extra, ((0, 0), (0, 0), (0, pad)))
    outgoing = jnp.concatenate([sent, extra], axis=-1)
    arrived = lax.all_to_all(outgoing, "ep", split_axis=0, concat_axis=0, tiled=True)
    arrived = arrived.reshape(ep_count * slots, -1)
    everyone = lax.all_gather(arrived, "tp", axis=0, tiled=True)
    produced = expert_layer(everyone, gate, up, down, arrived.shape[0])
    summed = lax.psum_scatter(produced, "tp", scatter_dimension=0, tiled=True)
    returned = lax.all_to_all(
        summed.reshape(ep_count, slots, width), "ep", split_axis=0, concat_axis=0, tiled=True
    )
    return jnp.einsum("tes,esd->td", spread, returned, preferred_element_type=f32).astype(bf16)


def by_weights(normed, expert_choice_index, mixing, gate, up, down):
    own_tokens, width_model = normed.shape
    ep_count = lax.axis_size("ep")
    local_experts = gate.shape[0]
    experts = local_experts * ep_count
    flat_ids = expert_choice_index.reshape(-1)
    one_hot = (flat_ids[:, None] == jnp.arange(experts, dtype=jnp.int32)[None, :]).astype(jnp.int32)
    slot_rank = jnp.sum((jnp.cumsum(one_hot, axis=0) - one_hot) * one_hot, axis=1)
    slot_index = flat_ids * CAP + slot_rank
    copy_token = jnp.arange(flat_ids.shape[0], dtype=jnp.int32) // TOPK
    slot_token = jnp.full((experts * CAP,), own_tokens, jnp.int32).at[slot_index].set(copy_token)
    outgoing = jnp.take(normed, slot_token, axis=0, mode="fill", fill_value=0).reshape(
        ep_count, local_experts, CAP, width_model
    )
    arrived = lax.all_to_all(outgoing, "ep", split_axis=0, concat_axis=0, tiled=True)
    gate_piece = lax.all_gather(gate, "tp", axis=1, tiled=True)
    up_piece = lax.all_gather(up, "tp", axis=1, tiled=True)
    down_piece = lax.all_gather(down, "tp", axis=1, tiled=True)
    gating = jnp.einsum("secd,efd->secf", arrived, gate_piece, preferred_element_type=jnp.float32)
    upward = jnp.einsum("secd,efd->secf", arrived, up_piece, preferred_element_type=jnp.float32)
    hidden = (jax.nn.silu(gating) * upward).astype(jnp.bfloat16)
    produced = jnp.einsum("secf,efd->secd", hidden, down_piece, preferred_element_type=jnp.float32)
    returned = lax.all_to_all(
        produced.astype(jnp.bfloat16), "ep", split_axis=0, concat_axis=0, tiled=True
    )
    flat_results = returned.reshape(experts * CAP, width_model)
    picked = (
        jnp.take(flat_results, slot_index, axis=0)
        .reshape(own_tokens, TOPK, width_model)
        .astype(jnp.float32)
    )
    return jnp.sum(mixing[..., None] * picked, axis=1).astype(jnp.bfloat16)


def compose(earlier, latter):
    joined_map = jnp.einsum("hij,hjk->hik", latter[0], earlier[0], precision=precise_setting)
    joined_state = (
        jnp.einsum("hij,hjv->hiv", latter[0], earlier[1], precision=precise_setting) + latter[1]
    )
    return (joined_map, joined_state)


def shards(
    query_heads_rows,
    key_heads_rows,
    value_heads_rows,
    write_strength_logit,
    decay_preactivation,
    head_decay_logarithm,
    extra_log_decay,
    output_weight,
    second_batch_tokens,
    expert_norm_scale,
    expert_choice_index,
    group_router_weight,
    expert_logit_difference,
    expert_gate_weight,
    expert_up_weight,
    expert_down_weight,
):
    length = query_heads_rows.shape[0]
    local_heads = head_decay_logarithm.shape[0]
    strength = jax.nn.sigmoid(write_strength_logit.astype(jnp.float32))
    decay_logarithm = (
        -jnp.exp(head_decay_logarithm)[:, None]
        * jax.nn.softplus(decay_preactivation.astype(jnp.float32))
        + extra_log_decay
    )
    local_output, projection_matrix, end_memory = delta_rule(
        query_heads_rows, key_heads_rows, value_heads_rows, strength, decay_logarithm
    )
    identity_map = jnp.broadcast_to(jnp.eye(DK, dtype=jnp.float32), (local_heads, DK, DK))
    carried_end = end_memory[..., :DV]
    transfer = end_memory[..., DV:]
    _, incoming_rows = prefix(
        (transfer, carried_end), "ep", compose, (identity_map, jnp.zeros_like(carried_end))
    )
    attention_result = local_output + jnp.einsum(
        "hpg,hgd->hpd", projection_matrix, incoming_rows, precision=precise_setting
    )
    attn_rows = (
        attention_result.transpose(1, 0, 2)
        .reshape(length, local_heads * DV)
        .astype(jnp.bfloat16)
    )
    summed = lax.psum_scatter(
        jnp.dot(attn_rows, output_weight, preferred_element_type=jnp.float32).astype(jnp.bfloat16),
        "tp",
        scatter_dimension=0,
        tiled=True,
    )
    widened = second_batch_tokens.astype(jnp.float32)
    normed = (
        widened
        * lax.rsqrt(jnp.mean(widened * widened, axis=-1, keepdims=True) + norm_eps)
        * expert_norm_scale
    ).astype(jnp.bfloat16)
    leading = jax.nn.sigmoid(expert_logit_difference)
    mixing = group_router_weight[:, None] * jnp.stack([leading, 1.0 - leading], axis=-1)
    local_experts, local_units, _ = expert_gate_weight.shape
    own_tokens = second_batch_tokens.shape[0]
    ep_count, tp_count = lax.axis_size("ep"), lax.axis_size("tp")
    named_both = TOPK if local_experts % EPG == 0 else 1
    slots = min(own_tokens, local_experts * CAP // named_both)
    weights = (expert_gate_weight, expert_up_weight, expert_down_weight)
    if 2 * tp_count * ep_count * slots < 3 * local_experts * local_units * tp_count:
        expert_out = by_tokens(normed, expert_choice_index, mixing, *weights, slots)
    else:
        expert_out = by_weights(normed, expert_choice_index, mixing, *weights)
    return (summed, expert_out)


def solution(mesh):
    in_specs = (
        P("ep", "tp"),
        P("ep", "tp"),
        P("ep", "tp"),
        P("tp", "ep"),
        P("tp", "ep"),
        P("tp"),
        P("tp", "ep"),
        P("tp", None),
        P(("ep", "tp"), None),
        P(),
        P(("ep", "tp"), None),
        P(("ep", "tp")),
        P(("ep", "tp")),
        P("ep", "tp", None),
        P("ep", "tp", None),
        P("ep", "tp", None),
    )
    out_specs = (P(("ep", "tp"), None), P(("ep", "tp"), None))
    return jax.shard_map(shards, mesh=mesh, in_specs=in_specs, out_specs=out_specs, check_vma=False)
```

time: 522 us -> 280 us (0.54)
  waiting for transfers between devices: 258 us -> 156 us
  other arithmetic: 98.3 us -> 4.24 us
  matrix products: 91.2 us -> 6.58 us
  Pallas kernels: 0 us -> 38.7 us
  blocking collectives: 22.5 us -> 56.8 us
  local copies, waits for them, and re-layouts: 26 us -> 2.72 us
  starting transfers between devices: 9.7 us -> 0.3 us
    all_gather x3 -> x1, waiting for transfers between devices: 231 us -> 86 us  [by_tokens(): everyone = lax.all_gather(arrived, 'tp', axis=0, tiled=True)]
    another operation x5 -> x0, other arithmetic: 81.1 us -> none  [the longest x2 80 us: block_terms(): jax.scipy.linalg.solve_triangular(system, rhs_cols, lower=True, unit_diag...]
    dot_general x38 -> x5, matrix products: 84.3 us -> 3.67 us  [the longest x1 1.56 us: by_tokens(): jnp.einsum('tes,td->esd', spread, normed, preferred_element_type=f32)]
    reduce_scatter x0 -> x1, waiting for transfers between devices: none -> 50 us  [by_tokens(): summed = lax.psum_scatter(produced, 'tp', scatter_dimension=0, tiled=True)]
    pallas_call x0 -> x2, Pallas kernels: none -> 38.7 us  [the longest x1 26 us: expert_layer(): pl.pallas_call(expert_kernel, grid=(count // tile,), out_shape=jax.ShapeD...]
    all_to_all x0 -> x2, blocking collectives: none -> 36.3 us  [the longest x1 20.2 us: by_tokens(): lax.all_to_all(outgoing, 'ep', split_axis=0, concat_axis=0, tiled=True)]
    all_to_all x2 -> x0, waiting for transfers between devices: 24.7 us -> none  [the longest x1 24.7 us: shards(): lax.all_to_all(produced.astype(jnp.bfloat16), 'ep', split_axis=0, concat_...]
    reduce_scatter x1, waiting for transfers between devices: 0.01 us -> 20.2 us  [shards(): lax.psum_scatter(jnp.dot(attn_rows, output_weight, preferred_element_type...]
  transfers between devices with their start and end apart: 6 -> 3, of which waited for: 3 -> 3; matrix products, arithmetic and copies ran while one was open for 41% -> 2% of each run, Pallas kernels for 0% -> 5%
where the time goes in v1:
time: 280 us
  waiting for transfers between devices  156 us (56%)
  blocking collectives  56.8 us (20%)
  Pallas kernels  38.7 us (14%)
  between operations  13.9 us (5%)
  matrix products  6.58 us (2%)
  other arithmetic  4.24 us (2%)
    all_gather x1, waiting for transfers between devices, by_tokens(): everyone = lax.all_gather(arrived, 'tp', axis=0, tiled=True)  86 us
    reduce_scatter x1, waiting for transfers between devices, by_tokens(): summed = lax.psum_scatter(produced, 'tp', scatter_dimension=0, tiled=True)  50 us
    pallas_call x1, Pallas kernels, expert_layer(): pl.pallas_call(expert_kernel, grid=(count // tile,), out_shape=jax.ShapeD...  26 us
    all_gather x2, blocking collectives, prefix(): pieces = jax.tree.map(lambda part: lax.all_gather(part, axis), value)  20.5 us
    all_to_all x1, blocking collectives, by_tokens(): lax.all_to_all(outgoing, 'ep', split_axis=0, concat_axis=0, tiled=True)  20.2 us
    reduce_scatter x1, waiting for transfers between devices, shards(): lax.psum_scatter(jnp.dot(attn_rows, output_weight, preferred_element_type...  20.2 us
    all_to_all x1, blocking collectives, by_tokens(): lax.all_to_all(summed.reshape(ep_count, slots, width), 'ep', split_axis=0...  16 us
    pallas_call x1, Pallas kernels, delta_rule(): pl.pallas_call(delta_kernel, out_shape=(jax.ShapeDtypeStruct((heads, leng...  12.7 us
  transfers between devices with their start and end apart: 3, of which 3 were waited for; matrix products, arithmetic and copies ran while one was open for 2% of the time, Pallas kernels for 5%

profile of v1, /device:TPU:0, one launch (start us, length us, event | category | flops | bytes accessed | tf_op | source)
XLA Modules:
  0.0 279.6 jit_solution(3816630038302392983)
XLA Ops:
  7.2 0.0 copy-start
  7.2 0.0 all-gather.4.cloned.1.call-start
  7.2 0.8 fusion.36
  8.0 0.7 subtract_bitcast_fusion
  8.7 0.7 maximum_multiply_fusion
  9.3 0.7 select_reduce_fusion
  10.1 0.2 fusion.31
  10.3 0.2 convolution_convert_fusion.2
  10.4 0.1 copy.45
  10.6 1.2 fusion.13
  11.8 1.6 convolution_convert_fusion.1
  13.4 0.1 fusion.12
  13.5 0.0 copy-start.1
  13.5 20.2 %all_to_all.10 = bf16[4,64,2176]{2,1,0:T(8,128)(2,1)} all-to-all(bf16[4,64,2176]{2,1,0:T(8,128)(2,1)S(1)} %fusion.12), channel_id=1, replica_groups=mesh['ep'=4,'tp'=8] {'ep'}, dimensions={0} | all-to-all | bytes 2228224 | tf_op jit(solution)/shard_map/all_to_all | solution.py:197
  33.7 0.0 all-gather.4.cloned.1.call-update
  33.8 0.0 reduce-scatter.5.cloned.1.call-start
  33.8 86.0 %all-gather.4.cloned.1.call-done.x_ref = bf16[2048,2176]{1,0:T(8,128)(2,1)} async-done(((bf16[256,2176]{1,0:T(8,128)(2,1)}), bf16[2048,2176]{1,0:T(8,128)(2,1)}) %all-gather.4.cloned.1.call-update) | async-done | bytes 8912912 | tf_op jit(solution)/shard_map/all_gather | solution.py:199
  119.8 0.0 copy-done.1
  119.8 0.0 copy-start.2
  119.8 1.6 copy-done.2
  121.4 26.0 %shard_map.168 = bf16[2048,2048]{1,0:T(8,128)(2,1)} custom-call(bf16[2048,2176]{1,0:T(8,128)(2,1)} %all-gather.4.cloned.1.call-done.x_ref, bf16[4,128,2048]{2,1,0:T(8,128)(2,1)S(1)} %copy-done.1, bf16[4,128,2048]{2,1,0:T(8,128)(2,1)S(1)} %copy-done.2, bf16[4,128,2048]{2,1,0:T(8,128)(2,1)} %down_ref.1), custom_call_target="tpu_custom_call" | custom-call | flops 12884901888 | bytes 23068672 | tf_op jit(solution)/shard_map/pallas_call | solution.py:155
  147.5 0.0 copy-start.9
  147.5 0.0 copy-start.6
  147.5 0.0 copy-start.7
  147.5 0.0 copy-start.8
  147.5 0.0 copy-start.3
  147.5 0.0 copy-start.4
  147.5 0.0 copy-start.5
  147.5 0.0 reduce-scatter.5.cloned.1.call-update
  147.5 0.2 reduce-scatter.3.cloned.1.call-start
  147.8 0.3 copy-done.9
  148.1 0.0 copy-done.6
  148.2 0.0 copy-done.7
  148.2 0.0 copy-done.8
  148.2 0.1 fusion.45
  148.3 0.2 copy-done.3
  148.5 0.1 copy-done.4
  148.6 0.1 copy-done.5
  148.6 12.7 %shard_map.167 = (f32[2,512,128]{2,1,0:T(8,128)S(1)}, f32[2,512,128]{2,1,0:T(8,128)S(1)}, f32[2,128,256]{2,1,0:T(8,128)S(1)}) custom-call(bf16[512,256]{1,0:T(8,128)(2,1)S(1)} %copy-done.3, bf16[512,256]{1,0:T(8,128)(2,1)S(1)} %copy-done.4, bf16[512,256]{1,0:T(8,128)(2,1)S(1)} %copy-done.5, f32[2,512]{1,0:T(2,128)S(1)} %get-tuple-element.138.strength_ref, ...), custom_call_target="tpu_custom_call" | custom-call | flops 4026531840 | bytes 4194304 | tf_op jit(solution)/shard_map/pallas_call | solution.py:115
  161.3 10.2 %all-gather = f32[8,128,128]{2,1,0:T(8,128)S(1)} all-gather(f32[2,128,128]{2,1,0:T(8,128)S(1)} %get-tuple-element.136), channel_id=2, replica_groups=mesh['ep'=4,'tp'=8] {'ep'}, dimensions={0}, use_global_device_ids=true | all-gather | bytes 655360 | tf_op jit(solution)/shard_map/all_gather | solution.py:21
  171.5 10.3 %all-gather.1 = f32[8,128,128]{2,1,0:T(8,128)S(1)} all-gather(f32[2,128,128]{2,1,0:T(8,128)S(1)} %get-tuple-element.135), channel_id=3, replica_groups=mesh['ep'=4,'tp'=8] {'ep'}, dimensions={0}, use_global_device_ids=true | all-gather | bytes 655360 | tf_op jit(solution)/shard_map/all_gather | solution.py:21
  181.8 0.9 while.14
  181.9 0.3 fusion.61
  182.2 0.3 fusion.61
  182.5 0.3 fusion.61
  182.8 0.6 fusion.11
  183.4 0.1 copy.41
  183.5 0.0 copy-done
  183.6 2.1 convolution_convert_fusion
  185.6 0.0 reduce-scatter.3.cloned.1.call-update
  185.7 50.0 %reduce-scatter.5.cloned.1.call-done = bf16[256,2048]{1,0:T(8,128)(2,1)} async-done(((bf16[2048,2048]{1,0:T(8,128)(2,1)}), bf16[256,2048]{1,0:T(8,128)(2,1)}) %reduce-scatter.5.cloned.1.call-update) | async-done | bytes 1048592 | tf_op jit(solution)/shard_map/reduce_scatter | solution.py:201
  235.7 16.0 %all_to_all.11 = bf16[4,64,2048]{2,1,0:T(8,128)(2,1)S(1)} all-to-all(bf16[4,64,2048]{2,1,0:T(8,128)(2,1)} %bitcast.38), channel_id=1, replica_groups=mesh['ep'=4,'tp'=8] {'ep'}, dimensions={0} | all-to-all | bytes 2097152 | tf_op jit(solution)/shard_map/all_to_all | solution.py:202
  251.7 1.2 fusion.8
  252.8 20.2 %reduce-scatter.3.cloned.1.call-done = bf16[64,2048]{1,0:T(8,128)(2,1)} async-done(((bf16[512,2048]{1,0:T(8,128)(2,1)}), bf16[64,2048]{1,0:T(8,128)(2,1)}) %reduce-scatter.3.cloned.1.call-update) | async-done | bytes 262160 | tf_op jit(solution)/shard_map/reduce_scatter | solution.py:293
  (10 shorter events, 0.1 us)
Async XLA Ops:
  7.2 176.4 %copy-start = (bf16[256,2048]{1,0:T(8,128)(2,1)S(1)}, bf16[256,2048]{1,0:T(8,128)(2,1)}, u32[]{:S(2)}) copy-start(bf16[256,2048]{1,0:T(8,128)(2,1)} %param.25) | copy-start | bytes 3145732
  7.2 112.7 %all-gather.4.cloned.1.call-start = ((), (), s32[]{:S(2)}) async-start(), calls=%async_computation.5 | async-start | bytes 10027008 | tf_op jit(solution)/shard_map/all_gather | solution.py:199
  13.5 106.4 %copy-start.1 = (bf16[4,128,2048]{2,1,0:T(8,128)(2,1)S(1)}, bf16[4,128,2048]{2,1,0:T(8,128)(2,1)}, u32[]{:S(2)}) copy-start(bf16[4,128,2048]{2,1,0:T(8,128)(2,1)} %gate_ref.1) | copy-start | bytes 6291460
  33.8 201.9 %reduce-scatter.5.cloned.1.call-start = ((), (), s32[]{:S(2)}) async-start(), calls=%async_computation.6 | async-start | bytes 9437184 | tf_op jit(solution)/shard_map/reduce_scatter | solution.py:201
  119.8 1.6 copy-start.2
  147.5 0.7 copy-start.9
  147.5 0.7 copy-start.6
  147.5 0.7 copy-start.7
  147.5 0.7 copy-start.8
  147.5 1.0 copy-start.3
  147.5 1.1 copy-start.4
  147.5 1.1 copy-start.5
  147.5 125.5 %reduce-scatter.3.cloned.1.call-start = ((), (), s32[]{:S(2)}) async-start(), calls=%async_computation.4 | async-start | bytes 2359296 | tf_op jit(solution)/shard_map/reduce_scatter | solution.py:293
Sparse Core Ops, SparseCore 0:
  33.9 85.9 all-gather.3
  147.7 87.9 reduce-scatter.4
  238.6 34.4 reduce-scatter.2

commit v2 on v1

--- a/solution.py
+++ b/solution.py
@@ -1,3 +1,5 @@
+import functools
+
 import jax
 import jax.numpy as jnp
 from jax import lax
@@ -8,6 +10,8 @@
 DK = 128
 DV = 128
 CAP = 32
+RING = 4
+MESH = pl.DeviceIdType.MESH
 EPG = 4
 TOPK = 2
 
@@ -16,18 +20,15 @@
 norm_eps = 1e-06
 
 
-def prefix(value, axis, join, neutral):
+def incoming(end_memory, axis):
     count, mine = (lax.axis_size(axis), lax.axis_index(axis))
-    pieces = jax.tree.map(lambda part: lax.all_gather(part, axis), value)
-    subtotal = jax.tree.map(
-        lambda part, zero: jnp.full_like(part, 0) + jnp.asarray(zero, part.dtype), value, neutral
-    )
-
-    def step(position, subtotal):
-        longer = join(subtotal, jax.tree.map(lambda part: part[position], pieces))
-        return jax.tree.map(lambda new, old: jnp.where(position < mine, new, old), longer, subtotal)
-
-    return lax.fori_loop(0, count - 1, step, subtotal)
+    pieces = lax.all_gather(end_memory, axis)
+    state = jnp.zeros(end_memory.shape[:-1] + (DV,), jnp.float32)
+    for position in range(count - 1):
+        end, transfer = pieces[position, ..., :DV], pieces[position, ..., DV:]
+        longer = end + jnp.einsum("hij,hjv->hiv", transfer, state, precision=precise_setting)
+        state = jnp.where(position < mine, longer, state)
+    return state
 
 
 def unit_rows(matrix):
@@ -167,7 +168,220 @@
     )(rows, gate, up, down)
 
 
-def by_tokens(normed, choice, mixing, gate, up, down, slots):
+def exchange_kernel(
+    ring, out_ref, spread_ref, gate_ref, up_ref, down_ref, result_ref,
+    rows, part, theirs, pair, passed, landed, onward, total, back,
+    local_sem, ep_sems, near_sems, far_sems, core_sems, pair_sems, half_sems, back_sems,
+):
+    e, t = lax.axis_index("ep"), lax.axis_index("tp")
+    peers, slots, _ = out_ref.shape
+    experts, units, width = gate_ref.shape
+    half = width // 2
+    core, z = lax.rem(t, 2), lax.div(t, 2)
+    bf16, f32 = jnp.bfloat16, jnp.float32
+
+    def at_chip(hop, same=True):
+        return lax.rem(z + hop, ring) * 2 + (core if same else 1 - core)
+
+    right, left, other = at_chip(1), at_chip(ring - 1), at_chip(0, False)
+
+    def at_peer(j):
+        return lax.rem(e + j, peers)
+
+    barrier = pltpu.get_barrier_semaphore()
+    greeted = [(at_peer(j), t) for j in range(1, peers)] + [(e, right), (e, left), (e, other)]
+    for device in greeted:
+        pl.semaphore_signal(barrier, inc=1, device_id=device, device_id_type=MESH)
+    pl.semaphore_wait(barrier, len(greeted))
+
+    started = []
+
+    def send(src, dst, sems, index, device):
+        copy = pltpu.make_async_remote_copy(
+            src_ref=src,
+            dst_ref=dst,
+            send_sem=sems.at[(0,) + index],
+            recv_sem=sems.at[(1,) + index],
+            device_id=device,
+            device_id_type=MESH,
+        )
+        copy.start()
+        started.append(copy)
+
+    def arrived(dst, sems, index):
+        pltpu.make_async_remote_copy(
+            src_ref=dst,
+            dst_ref=dst,
+            send_sem=sems.at[(0,) + index],
+            recv_sem=sems.at[(1,) + index],
+            device_id=(e, other),
+            device_id_type=MESH,
+        ).wait_recv()
+
+    own = pltpu.make_async_copy(out_ref.at[e], rows.at[t, e], local_sem)
+    own.start()
+    for j in range(1, peers):
+        target = at_peer(j)
+        send(out_ref.at[target], rows.at[t, e], ep_sems, (j,), (target, t))
+    sources = [lax.rem(e + peers - j, peers) for j in range(peers)]
+
+    def piece(hop, j, same=True):
+        return rows.at[at_chip(hop, same), sources[j]]
+
+    def to_other(hop, j):
+        send(piece(hop, j), piece(hop, j), core_sems, (hop, j), (e, other))
+
+    def own_piece(j):
+        if j == 0:
+            own.wait()
+        else:
+            arrived(piece(0, j), ep_sems, (j,))
+        send(piece(0, j), piece(0, j), near_sems, (0, j), (e, right))
+        send(piece(0, j), piece(0, j), near_sems, (1, j), (e, left))
+        to_other(0, j)
+
+    def near_piece(j):
+        arrived(piece(ring - 1, j), near_sems, (0, j))
+        if j % 2 == 0:
+            send(piece(ring - 1, j), piece(ring - 1, j), far_sems, (j,), (e, right))
+        arrived(piece(1, j), near_sems, (1, j))
+        if j % 2 == 1:
+            send(piece(1, j), piece(1, j), far_sems, (j,), (e, left))
+        to_other(ring - 1, j)
+        to_other(1, j)
+
+    def far_piece(j):
+        arrived(piece(2, j), far_sems, (j,))
+        to_other(2, j)
+
+    def produce(hop):
+        for j in range(peers):
+            arrived(piece(hop, j, False), core_sems, (hop, j))
+
+        def one(k, carry):
+            which = lax.rem(core + 1 + k, 2)
+            block = rows[lax.rem(z + hop, ring) * 2 + which].reshape(peers * slots, -1)
+            x = block[:, :width]
+            hidden = []
+            for n in range(experts):
+                gating = lax.dot_general(
+                    x, gate_ref[n], (((1,), (1,)), ((), ())), preferred_element_type=f32
+                )
+                upward = lax.dot_general(
+                    x, up_ref[n], (((1,), (1,)), ((), ())), preferred_element_type=f32
+                )
+                share = block[:, width + n : width + n + 1].astype(f32) + block[
+                    :, width + experts + n : width + experts + n + 1
+                ].astype(f32)
+                hidden.append((gating / (1.0 + jnp.exp(-gating)) * upward * share).astype(bf16))
+            hidden = jnp.concatenate(hidden, axis=1)
+            down = down_ref[...].reshape(experts * units, width)
+            for h in range(2):
+                part[hop, k, h] = jnp.dot(
+                    hidden, down[:, h * half : (h + 1) * half], preferred_element_type=f32
+                ).astype(bf16)
+            return carry
+
+        lax.fori_loop(0, 2, one, 0)
+        send(part.at[hop, 0], theirs.at[hop], pair_sems, (hop,), (e, other))
+
+    def join(hop):
+        arrived(theirs.at[hop], pair_sems, (hop,))
+        for h in range(2):
+            pair[hop, h] = (part[hop, 1, h].astype(f32) + theirs[hop, h].astype(f32)).astype(bf16)
+
+    for j in range(peers):
+        own_piece(j)
+        if j >= 1:
+            near_piece(j - 1)
+        if j >= 2:
+            far_piece(j - 2)
+    produce(0)
+    near_piece(peers - 1)
+    join(0)
+    far_piece(peers - 2)
+    produce(1)
+    produce(ring - 1)
+    far_piece(peers - 1)
+    join(1)
+    send(pair.at[1, 1], landed.at[0, 1], half_sems, (0, 1), (e, right))
+    join(ring - 1)
+    send(pair.at[ring - 1, 0], landed.at[1, 0], half_sems, (1, 0), (e, left))
+    produce(2)
+    join(2)
+    send(pair.at[2, 0], passed.at[0], half_sems, (2, 0), (e, right))
+    send(pair.at[2, 1], passed.at[1], half_sems, (2, 1), (e, left))
+    arrived(passed.at[0], half_sems, (2, 0))
+    onward[0] = (pair[1, 0].astype(f32) + passed[0].astype(f32)).astype(bf16)
+    send(onward.at[0], landed.at[0, 0], half_sems, (0, 0), (e, right))
+    arrived(passed.at[1], half_sems, (2, 1))
+    onward[1] = (pair[ring - 1, 1].astype(f32) + passed[1].astype(f32)).astype(bf16)
+    send(onward.at[1], landed.at[1, 1], half_sems, (1, 1), (e, left))
+    for h in range(2):
+        arrived(landed.at[h, 1 - h], half_sems, (h, 1 - h))
+    for h in range(2):
+        arrived(landed.at[h, h], half_sems, (h, h))
+        summed = pair[0, h].astype(f32) + landed[0, h].astype(f32) + landed[1, h].astype(f32)
+        total[h] = summed.astype(bf16).reshape(peers, slots, half)
+        for j in range(1, peers):
+            target = at_peer(j)
+            send(total.at[h, target], back.at[h, e], back_sems, (h, j), (target, t))
+        back[h, e] = total[h, e]
+    for h in range(2):
+        for j in range(1, peers):
+            arrived(back.at[h, sources[j]], back_sems, (h, j))
+        result_ref[:, h * half : (h + 1) * half] = jnp.dot(
+            spread_ref[...], back[h].reshape(peers * slots, half), preferred_element_type=f32
+        ).astype(bf16)
+    for copy in started:
+        copy.wait_send()
+
+
+def exchange(outgoing, spread, gate, up, down, ring):
+    peers, slots, wide = outgoing.shape
+    _, _, width = gate.shape
+    count, half = peers * slots, width // 2
+    bf16 = jnp.bfloat16
+    vmem = pl.BlockSpec(memory_space=pltpu.VMEM)
+    dma = pltpu.SemaphoreType.DMA
+    experts, units, _ = gate.shape
+    total_rows = 2 * ring * count
+    return pl.pallas_call(
+        functools.partial(exchange_kernel, ring),
+        out_shape=jax.ShapeDtypeStruct((spread.shape[0], width), bf16),
+        in_specs=[vmem] * 5,
+        out_specs=vmem,
+        scratch_shapes=[
+            pltpu.VMEM((2 * ring, peers, slots, wide), bf16),
+            pltpu.VMEM((ring, 2, 2, count, half), bf16),
+            pltpu.VMEM((ring, 2, count, half), bf16),
+            pltpu.VMEM((ring, 2, count, half), bf16),
+            pltpu.VMEM((2, count, half), bf16),
+            pltpu.VMEM((2, 2, count, half), bf16),
+            pltpu.VMEM((2, count, half), bf16),
+            pltpu.VMEM((2, peers, slots, half), bf16),
+            pltpu.VMEM((2, peers, slots, half), bf16),
+            dma,
+            dma((2, peers)),
+            dma((2, 2, peers)),
+            dma((2, peers)),
+            dma((2, ring, peers)),
+            dma((2, ring)),
+            dma((2, 3, 2)),
+            dma((2, 2, peers)),
+        ],
+        cost_estimate=pl.CostEstimate(
+            flops=60 * total_rows * experts * units * width,
+            bytes_accessed=6 * experts * units * width,
+            transcendentals=0,
+        ),
+        compiler_params=pltpu.CompilerParams(
+            collective_id=0, has_side_effects=True, vmem_limit_bytes=60 * 2**20
+        ),
+    )(outgoing, spread, gate, up, down)
+
+
+def by_tokens(normed, choice, mixing, gate, up, down, slots, after):
     ep_count = lax.axis_size("ep")
     local_experts = gate.shape[0]
     tokens, width = normed.shape
@@ -194,6 +408,10 @@
     pad = -extra.shape[-1] % 128
     extra = jnp.pad(extra, ((0, 0), (0, 0), (0, pad)))
     outgoing = jnp.concatenate([sent, extra], axis=-1)
+    if lax.axis_size("tp") == 2 * RING and ep_count > 1:
+        outgoing, after = lax.optimization_barrier((outgoing, after))
+        flat = spread.reshape(tokens, ep_count * slots)
+        return exchange(outgoing, flat, gate, up, down, RING), after
     arrived = lax.all_to_all(outgoing, "ep", split_axis=0, concat_axis=0, tiled=True)
     arrived = arrived.reshape(ep_count * slots, -1)
     everyone = lax.all_gather(arrived, "tp", axis=0, tiled=True)
@@ -202,7 +420,8 @@
     returned = lax.all_to_all(
         summed.reshape(ep_count, slots, width), "ep", split_axis=0, concat_axis=0, tiled=True
     )
-    return jnp.einsum("tes,esd->td", spread, returned, preferred_element_type=f32).astype(bf16)
+    combined = jnp.einsum("tes,esd->td", spread, returned, preferred_element_type=f32)
+    return combined.astype(bf16), after
 
 
 def by_weights(normed, expert_choice_index, mixing, gate, up, down):
@@ -237,14 +456,6 @@
         .astype(jnp.float32)
     )
     return jnp.sum(mixing[..., None] * picked, axis=1).astype(jnp.bfloat16)
-
-
-def compose(earlier, latter):
-    joined_map = jnp.einsum("hij,hjk->hik", latter[0], earlier[0], precision=precise_setting)
-    joined_state = (
-        jnp.einsum("hij,hjv->hiv", latter[0], earlier[1], precision=precise_setting) + latter[1]
-    )
-    return (joined_map, joined_state)
 
 
 def shards(
@@ -276,12 +487,7 @@
     local_output, projection_matrix, end_memory = delta_rule(
         query_heads_rows, key_heads_rows, value_heads_rows, strength, decay_logarithm
     )
-    identity_map = jnp.broadcast_to(jnp.eye(DK, dtype=jnp.float32), (local_heads, DK, DK))
-    carried_end = end_memory[..., :DV]
-    transfer = end_memory[..., DV:]
-    _, incoming_rows = prefix(
-        (transfer, carried_end), "ep", compose, (identity_map, jnp.zeros_like(carried_end))
-    )
+    incoming_rows = incoming(end_memory, "ep")
     attention_result = local_output + jnp.einsum(
         "hpg,hgd->hpd", projection_matrix, incoming_rows, precision=precise_setting
     )
@@ -290,12 +496,8 @@
         .reshape(length, local_heads * DV)
         .astype(jnp.bfloat16)
     )
-    summed = lax.psum_scatter(
-        jnp.dot(attn_rows, output_weight, preferred_element_type=jnp.float32).astype(jnp.bfloat16),
-        "tp",
-        scatter_dimension=0,
-        tiled=True,
-    )
+    product = jnp.dot(attn_rows, output_weight, preferred_element_type=jnp.float32)
+    product = product.astype(jnp.bfloat16)
     widened = second_batch_tokens.astype(jnp.float32)
     normed = (
         widened
@@ -311,9 +513,12 @@
     slots = min(own_tokens, local_experts * CAP // named_both)
     weights = (expert_gate_weight, expert_up_weight, expert_down_weight)
     if 2 * tp_count * ep_count * slots < 3 * local_experts * local_units * tp_count:
-        expert_out = by_tokens(normed, expert_choice_index, mixing, *weights, slots)
+        expert_out, product = by_tokens(
+            normed, expert_choice_index, mixing, *weights, slots, product
+        )
     else:
         expert_out = by_weights(normed, expert_choice_index, mixing, *weights)
+    summed = lax.psum_scatter(product, "tp", scatter_dimension=0, tiled=True)
     return (summed, expert_out)
 
 

time: 280 us -> 253 us (0.904)
  Pallas kernels: 38.7 us -> 197 us
  waiting for transfers between devices: 156 us -> 25.7 us
  blocking collectives: 56.8 us -> 0 us
    pallas_call x1, Pallas kernels: 26 us -> 184 us  [exchange(): pl.pallas_call(functools.partial(exchange_kernel, ring), out_shape=jax.Sh...]
    reduce_scatter x2 -> x1, waiting for transfers between devices: 70.2 us -> 0.02 us  [shards(): summed = lax.psum_scatter(product, 'tp', scatter_dimension=0, tiled=True)]
    all_gather x1, waiting for transfers between devices: 86 us -> 25.6 us  [incoming(): pieces = lax.all_gather(end_memory, axis)]
    all_to_all x2 -> x0, blocking collectives: 36.3 us -> none  [the longest x1 20.2 us: by_tokens(): lax.all_to_all(outgoing, 'ep', split_axis=0, concat_axis=0, tiled=True)]
    all_gather x2 -> x0, blocking collectives: 20.5 us -> none  [prefix(): pieces = jax.tree.map(lambda part: lax.all_gather(part, axis), value)]
  transfers between devices with their start and end apart: 3 -> 2, of which waited for: 3 -> 1; matrix products, arithmetic and copies ran while one was open for 2% -> 1% of each run, Pallas kernels for 5% -> 73%
where the time goes in v2:
time: 253 us
  Pallas kernels  197 us (78%)
  waiting for transfers between devices  25.7 us (10%)
  between operations  14.2 us (6%)
  matrix products  7.24 us (3%)
  local copies, waits for them, and re-layouts  5.37 us (2%)
  other arithmetic  3.56 us (1%)
    pallas_call x1, Pallas kernels, exchange(): pl.pallas_call(functools.partial(exchange_kernel, ring), out_shape=jax.Sh...  184 us
    all_gather x1, waiting for transfers between devices, incoming(): pieces = lax.all_gather(end_memory, axis)  25.6 us
    pallas_call x1, Pallas kernels, delta_rule(): pl.pallas_call(delta_kernel, out_shape=(jax.ShapeDtypeStruct((heads, leng...  13.2 us
  transfers between devices with their start and end apart: 2, of which 1 were waited for; matrix products, arithmetic and copies ran while one was open for 1% of the time, Pallas kernels for 73%

profile of v2, /device:TPU:0, one launch (start us, length us, event | category | flops | bytes accessed | tf_op | source)
XLA Modules:
  0.0 253.0 jit_solution(12986508239495365747)
XLA Ops:
  7.2 0.0 copy-start
  7.2 0.0 all-gather.3.cloned.1.call-start
  7.2 0.7 exponential_negate_fusion
  8.0 0.8 fusion.37
  8.7 0.0 copy-start.1
  8.8 1.0 copy-done.1
  9.7 0.0 copy-start.2
  9.7 0.9 copy-done.2
  10.7 0.0 copy-start.3
  10.7 0.9 copy-done.3
  11.6 0.0 copy-start.6
  11.6 0.0 copy-start.8
  11.6 0.0 copy-start.7
  11.6 0.0 copy-start.4
  11.6 0.0 copy-start.5
  11.6 13.2 %shard_map.167 = (f32[2,512,128]{2,1,0:T(8,128)S(1)}, f32[2,512,128]{2,1,0:T(8,128)S(1)}, f32[2,128,256]{2,1,0:T(8,128)}) custom-call(bf16[512,256]{1,0:T(8,128)(2,1)S(1)} %copy-done.1, bf16[512,256]{1,0:T(8,128)(2,1)S(1)} %copy-done.2, bf16[512,256]{1,0:T(8,128)(2,1)S(1)} %copy-done.3, f32[2,512]{1,0:T(2,128)S(1)} %get-tuple-element.17.strength_ref, ...), custom_call_target="tpu_custom_call" | custom-call | flops 4026531840 | bytes 4194304 | tf_op jit(solution)/shard_map/pallas_call | solution.py:116
  24.8 0.0 all-gather.3.cloned.1.call-update
  24.8 0.2 reduce-scatter.2.cloned.1.call-start
  25.0 0.0 copy-done.6
  25.1 0.0 copy-done.8
  25.1 0.0 copy-done.7
  25.2 0.2 fusion.23
  25.4 0.2 convolution_convert_fusion.2
  25.5 0.1 copy.47
  25.7 0.1 copy.52
  25.9 0.1 copy.51
  26.0 0.1 eq.45
  26.1 0.0 copy-done.4
  26.1 0.2 fusion.7
  26.3 0.7 and_convert_fusion.spread_ref
  26.9 0.0 copy-done.5
  26.9 0.5 convolution_convert_fusion.1
  27.4 1.1 fusion.6.out_ref
  28.6 25.6 %all-gather.3.cloned.1.call-done = f32[8,128,256]{2,1,0:T(8,128)} async-done(((f32[2,128,256]{2,1,0:T(8,128)}), f32[8,128,256]{2,1,0:T(8,128)}) %all-gather.3.cloned.1.call-update) | async-done | bytes 1048592 | tf_op jit(solution)/shard_map/all_gather | solution.py:25
  54.2 1.2 fusion.5
  55.4 1.2 fusion.4
  56.7 1.2 fusion.3
  57.9 0.6 fusion.2
  58.5 0.1 copy.50
  58.6 0.0 copy-done
  58.7 2.1 convolution_convert_fusion
  60.7 0.0 reduce-scatter.2.cloned.1.call-update
  60.7 183.5 %shard_map.168 = bf16[128,2048]{1,0:T(8,128)(2,1)} custom-call(bf16[4,64,2176]{2,1,0:T(8,128)(2,1)} %fusion.6.out_ref, bf16[128,256]{1,0:T(8,128)(2,1)} %and_convert_fusion.spread_ref, bf16[4,128,2048]{2,1,0:T(8,128)(2,1)} %gate_ref.1, bf16[4,128,2048]{2,1,0:T(8,128)(2,1)} %up_ref.1, bf16[4,128,2048]{2,1,0:T(8,128)(2,1)} %down_ref.1), custom_call_target="tpu_custom_call" | custom-call | flops 128849018880 | bytes 6291456 | tf_op jit(solution)/shard_map/pallas_call | solution.py:349
  244.3 0.0 reduce-scatter.2.cloned.1.call-done
  244.3 1.9 copy.56
  (11 shorter events, 0.1 us)
Async XLA Ops:
  7.2 51.5 %copy-start = (bf16[256,2048]{1,0:T(8,128)(2,1)S(1)}, bf16[256,2048]{1,0:T(8,128)(2,1)}, u32[]{:S(2)}) copy-start(bf16[256,2048]{1,0:T(8,128)(2,1)} %param.23) | copy-start | bytes 3145732
  7.2 47.0 %all-gather.3.cloned.1.call-start = ((), (), s32[]{:S(2)}) async-start(), calls=%async_computation.2 | async-start | bytes 1310720 | tf_op jit(solution)/shard_map/all_gather | solution.py:25
  8.7 1.0 copy-start.1
  9.7 0.9 copy-start.2
  10.7 0.9 copy-start.3
  11.6 13.4 %copy-start.6 = (s32[128,2]{0,1:T(2,128)S(1)}, s32[128,2]{0,1:T(2,128)}, u32[]{:S(2)}) copy-start(s32[128,2]{0,1:T(2,128)} %param.26) | copy-start | bytes 3076
  11.6 13.5 %copy-start.8 = (f32[128]{0:T(128)S(1)}, f32[128]{0:T(128)}, u32[]{:S(2)}) copy-start(f32[128]{0:T(128)} %param.28) | copy-start | bytes 1540
  11.6 13.5 %copy-start.7 = (f32[128]{0:T(128)S(1)}, f32[128]{0:T(128)}, u32[]{:S(2)}) copy-start(f32[128]{0:T(128)} %param.27) | copy-start | bytes 1540
  11.6 14.4 %copy-start.4 = (bf16[128,2048]{1,0:T(8,128)(2,1)S(1)}, bf16[128,2048]{1,0:T(8,128)(2,1)}, u32[]{:S(2)}) copy-start(bf16[128,2048]{1,0:T(8,128)(2,1)} %param.24) | copy-start | bytes 1572868
  11.6 15.3 %copy-start.5 = (f32[2048]{0:T(1024)S(1)}, f32[2048]{0:T(1024)}, u32[]{:S(2)}) copy-start(f32[2048]{0:T(1024)} %param.25) | copy-start | bytes 24580
  24.8 219.5 %reduce-scatter.2.cloned.1.call-start = ((), (), s32[]{:S(2)}) async-start(), calls=%async_computation.1 | async-start | bytes 2359296 | tf_op jit(solution)/shard_map/reduce_scatter | solution.py:521
Sparse Core Ops, SparseCore 0:
  24.9 29.2 all-gather.2
  60.9 69.1 reduce-scatter.1
